TPU v7x, 32 devices: a whole 2x2x4 slice. The times are simulated.
32 devices in a mesh: sp: 8 (over z, y), tp: 4 (over x, core).
Axes of the slice: x: 2, y: 2, z: 4, core: 2. Of those that a mesh axis runs over, the one named last changes fastest.
Arguments:
- tokens: bfloat16 [4096, 2048], P(('sp', 'tp')), may hold values from -6 to 6
- norm_gain: bfloat16 [2048], replicated, may hold values from 0.099609375 to 1.8984375
- proj_x: bfloat16 [2048, 2048], P('sp', 'tp'), may hold values from -0.125 to 0.125
- gate_projection: bfloat16 [2048, 2048], P('sp', 'tp'), may hold values from -0.125 to 0.125
- conv_taps: bfloat16 [4, 2048], P(None, 'tp'), may hold values from -3 to 3
- gate_recur: bfloat16 [8, 256, 256], P('tp'), may hold values from -0.375 to 0.375
- gate_input: bfloat16 [8, 256, 256], P('tp'), may hold values from -0.375 to 0.375
- decay_param: float32 [2048], P('tp'), may hold values from 4 to 25
- decay_shift: float32 [8, 4096], P('tp', 'sp'), may hold values from -1.3 to 0, as said below
- proj_out: bfloat16 [2048, 2048], P('tp', 'sp'), may hold values from -0.125 to 0.125
Outputs:
- mixed_out: bfloat16 [4096, 2048], P(('sp', 'tp'))
Inputs may be any that keep to these rules, and one draw needn't show every extreme that they name: `decay_shift`: added log-decays, never positive.
All inputs are finite; a program needn't handle non-finite values.
Results may differ from a plain program's by a relative error of at most 0.015.
Values may be sent and summed in bfloat16 or wider, within the bound.
A program may use at most 128 MiB of HBM per device.

v0:
```python
import jax
import jax.numpy as jnp
from jax import lax
from jax.sharding import PartitionSpec as P

HEAD = 256
CONV = 4


def shifted(block, axis, distance):
    devices = range(lax.axis_size(axis))
    route = [(i - distance, i) for i in devices if i - distance in devices]
    return lax.ppermute(block, axis, route)


def carried_in(array, axis, combine, identity):
    size, index = (lax.axis_size(axis), lax.axis_index(axis))
    everything = jax.tree.map(lambda part: lax.all_gather(part, axis), array)
    start = jax.tree.map(
        lambda part, zero: jnp.broadcast_to(jnp.asarray(zero, part.dtype), part.shape),
        array,
        identity,
    )

    def turn(k, before):
        reached = k < index
        new = combine(before, jax.tree.map(lambda part: part[k], everything))
        return jax.tree.map(lambda a, b: jnp.where(reached, a, b), new, before)

    return lax.fori_loop(0, size, turn, start)


def rms_norm(values, norm_gain):
    floats = values.astype(jnp.float32)
    scaled = floats * lax.rsqrt(jnp.mean(floats * floats, axis=-1, keepdims=True) + 1e-06)
    return (scaled * norm_gain.astype(jnp.float32)).astype(jnp.bfloat16)


def combine_pair(earlier, later):
    return (earlier[0] * later[0], later[0] * earlier[1] + later[1])


def on_device(
    tokens,
    norm_gain,
    proj_x,
    gate_projection,
    conv_taps,
    gate_recur,
    gate_input,
    decay_param,
    decay_shift,
    proj_out,
):
    normed = rms_norm(tokens, norm_gain)
    full_x, full_gate = (
        lax.all_gather(proj_x, "sp", axis=0, tiled=True),
        lax.all_gather(gate_projection, "sp", axis=0, tiled=True),
    )
    local_width = proj_x.shape[1]
    piece = lax.all_gather(normed, "tp", axis=0, tiled=True)
    branch_piece = jnp.dot(piece, full_x, preferred_element_type=jnp.float32).astype(jnp.bfloat16)
    gating_piece = jnp.dot(piece, full_gate, preferred_element_type=jnp.float32).astype(
        jnp.bfloat16
    )
    joined = jnp.concatenate([branch_piece, gating_piece], axis=1)
    branch = joined[:, :local_width]
    gating = joined[:, local_width:]
    row_count = branch.shape[0]
    tail_rows = shifted(branch[row_count - CONV + 1 :], "sp", 1)
    extended = jnp.concatenate([tail_rows, branch], axis=0)
    conv_sum = jnp.zeros((row_count, local_width), jnp.float32)
    for tap_index in range(CONV):
        conv_sum = conv_sum + extended[tap_index : tap_index + row_count].astype(
            jnp.float32
        ) * conv_taps[tap_index].astype(jnp.float32)
    conved = conv_sum.astype(jnp.bfloat16)
    head_count = gate_recur.shape[0]
    grouped = conved.reshape(row_count, head_count, HEAD)
    recur = jax.nn.sigmoid(
        jnp.einsum("thi,hij->thj", grouped, gate_recur, preferred_element_type=jnp.float32)
    )
    inlet = jax.nn.sigmoid(
        jnp.einsum("thi,hij->thj", grouped, gate_input, preferred_element_type=jnp.float32)
    )
    decay_rate = jax.nn.softplus(-decay_param).reshape(head_count, HEAD)
    log_decay = (-8.0 * recur * decay_rate[None] + jnp.transpose(decay_shift)[:, :, None]).reshape(
        row_count, local_width
    )
    decay = jnp.exp(log_decay)
    drive = (
        jnp.sqrt(-jnp.expm1(2.0 * log_decay))
        * inlet.reshape(row_count, local_width)
        * conved.astype(jnp.float32)
    )
    identity = (jnp.ones((local_width,), jnp.float32), jnp.zeros((local_width,), jnp.float32))
    cumulative, local_state = lax.associative_scan(combine_pair, (decay, drive), axis=0)
    carried = carried_in(
        (cumulative[row_count - 1], local_state[row_count - 1]), "sp", combine_pair, identity
    )
    states = local_state + cumulative * carried[1][None, :]
    mixed = (states * jax.nn.gelu(gating.astype(jnp.float32))).astype(jnp.bfloat16)
    out_cols = lax.all_gather(proj_out, "sp", axis=1, tiled=True)
    return lax.psum_scatter(
        jnp.dot(mixed, out_cols, preferred_element_type=jnp.float32).astype(jnp.bfloat16),
        "tp",
        scatter_dimension=0,
        tiled=True,
    )


def solution(mesh):
    in_specs = (
        P(("sp", "tp"), None),
        P(),
        P("sp", "tp"),
        P("sp", "tp"),
        P(None, "tp"),
        P("tp", None, None),
        P("tp", None, None),
        P("tp"),
        P("tp", "sp"),
        P("tp", "sp"),
    )
    out_specs = P(("sp", "tp"), None)
    return jax.shard_map(
        on_device, mesh=mesh, in_specs=in_specs, out_specs=out_specs, check_vma=False
    )
```

profile of v0, /device:TPU:0, one launch (start us, length us, event | category | flops | bytes accessed | tf_op | source)
XLA Modules:
  0.0 287.4 jit_solution(4033228351637639462)
XLA Ops:
  6.5 1.3 fusion.11
  7.8 0.7 convert_element_type.51
  8.5 2.0 fusion.13
  10.6 0.7 all-gather.9.cloned.1.call-update
  11.4 0.7 all-gather.11.cloned.1.call-update
  12.1 0.5 all-gather.13.cloned.1.call-update
  12.7 23.3 %all-gather.7.cloned.1.call-done = bf16[512,2048]{1,0:T(8,128)(2,1)} async-done(((bf16[128,2048]{1,0:T(8,128)(2,1)}), bf16[512,2048]{1,0:T(8,128)(2,1)}) %all-gather.7.cloned.1.call-update) | async-done | bytes 2097168 | tf_op jit(solution)/shard_map/all_gather | solution.py:61
  36.0 51.2 %all-gather.9.cloned.1.call-done = bf16[2048,512]{1,0:T(8,128)(2,1)} async-done(((bf16[256,512]{1,0:T(8,128)(2,1)}), bf16[2048,512]{1,0:T(8,128)(2,1)}) %all-gather.9.cloned.1.call-update) | async-done | bytes 2097168 | tf_op jit(solution)/shard_map/all_gather | solution.py:57
  87.3 3.5 %convolution_convert_fusion.2 = bf16[512,512]{1,0:T(8,128)(2,1)S(1)} fusion(bf16[512,2048]{1,0:T(8,128)(2,1)} %all-gather.7.cloned.1.call-done, bf16[2048,512]{1,0:T(8,128)(2,1)} %all-gather.9.cloned.1.call-done), kind=kOutput, calls=%fused_computation.24 | convolution fusion | flops 1074003968 | bytes 4718592 | tf_op jit(solution)/shard_map/dot_general | solution.py:62
  90.7 2.5 collective-permute-start
  93.3 1.2 collective-permute-done
  94.5 0.5 add_convert_fusion
  95.1 0.6 fusion.49
  95.7 0.1 copy-done.2
  95.8 0.4 copy-done.11
  96.2 1.9 fusion.4
  98.1 1.6 copy.31
  99.7 1.2 convert_multiply_fusion.5
  100.9 2.3 slice.367
  103.2 2.1 slice.305
  105.3 2.1 slice.304
  107.3 0.2 slice_reduce_fusion
  107.5 19.5 %slice.303 = f32[256,512]{0,1:T(8,128)S(1)} slice(f32[512,512]{0,1:T(8,128)S(1)} %bitcast.49), slice={[1:512:2], [0:512:1]} | slice | bytes 1048576 | tf_op jit(solution)/shard_map/slice | solution.py:97
  127.0 19.4 %slice.302 = f32[255,512]{0,1:T(8,128)S(1)} slice(f32[512,512]{0,1:T(8,128)S(1)} %bitcast.50), slice={[2:512:2], [0:512:1]} | slice | bytes 1044480 | tf_op jit(solution)/shard_map/slice | solution.py:97
  146.4 19.5 %slice.307 = f32[256,512]{0,1:T(8,128)S(1)} slice(f32[512,512]{0,1:T(8,128)S(1)} %bitcast.51), slice={[0:511:2], [0:512:1]} | slice | bytes 1048576 | tf_op jit(solution)/shard_map/slice | solution.py:97
  165.9 1.0 copy.36
  166.9 0.2 copy.37
  167.1 0.1 copy-done.4
  167.3 1.3 multiply_add_fusion
  168.5 0.3 slice.365
  168.9 0.3 slice.311
  169.2 0.3 slice.310
  169.6 0.3 slice.313
  169.9 0.3 slice.309
  170.2 0.3 slice.308
  170.6 0.1 multiply_add_fusion.1
  170.7 0.2 slice.363
  170.9 0.1 slice.317
  171.0 0.1 slice.316
  171.1 0.1 slice.319
  171.2 0.1 slice.315
  171.3 0.4 slice.314
  172.7 1.0 copy.35
  174.9 0.2 fusion.33
  175.1 0.1 pad.142
  175.2 0.1 pad.124
  175.3 0.1 pad.125
  175.4 0.1 pad.143
  175.5 0.1 add.303
  175.6 0.1 add.293
  175.7 0.9 copy-done.5
  176.5 0.2 copy-done.6
  176.7 1.2 fusion.25
  177.9 2.9 pad.144
  180.8 2.7 pad.126
  183.6 2.7 pad.127
  186.3 0.7 add_bitcast_fusion
  187.0 27.3 %all-gather.1 = f32[8,1,512]{2,1,0:T(1,128)S(1)} all-gather(f32[1,1,512]{2,1,0:T(1,128)S(1)} %add_bitcast_fusion), channel_id=1, replica_groups=mesh['sp'=8,'tp'=4] {'sp'}, dimensions={0}, use_global_device_ids=true | all-gather | bytes 18432 | tf_op jit(solution)/shard_map/all_gather | solution.py:18
  214.3 2.8 pad.145
  217.1 0.7 add_bitcast_fusion.1
  217.8 26.1 %all-gather = f32[8,1,512]{2,1,0:T(1,128)S(1)} all-gather(f32[1,1,512]{2,1,0:T(1,128)S(1)} %add_bitcast_fusion.1), channel_id=1, replica_groups=mesh['sp'=8,'tp'=4] {'sp'}, dimensions={0}, use_global_device_ids=true | all-gather | bytes 18432 | tf_op jit(solution)/shard_map/all_gather | solution.py:18
  243.9 0.4 while.14
  244.4 7.9 %convolution_convert_fusion = bf16[512,2048]{1,0:T(8,128)(2,1)} fusion(bf16[512,2048]{1,0:T(8,128)(2,1)} %all-gather.13.cloned.1.call-done, bf16[512,2048]{1,0:T(8,128)(2,1)} %all-gather.7.cloned.1.call-done, bf16[2048,512]{1,0:T(8,128)(2,1)} %all-gather.11.cloned.1.call-done, f32[512,512]{1,0:T(8,128)S(1)} %copy-done.8, f32[512,512]{1,0:T(8,128)} %pad.145, ...), kind=kOutput, calls=%fused_computation.3 | convolution fusion | flops 2152726528 | bytes 12584960 | tf_op jit(solution)/shard_map/dot_general | solution.py:105
  252.3 28.5 %reduce-scatter.2.cloned.1.call-done = bf16[128,2048]{1,0:T(8,128)(2,1)} async-done(((bf16[512,2048]{1,0:T(8,128)(2,1)}), bf16[128,2048]{1,0:T(8,128)(2,1)}) %reduce-scatter.2.cloned.1.call-update) | async-done | bytes 524304 | tf_op jit(solution)/shard_map/reduce_scatter | solution.py:104
  (162 shorter events, 2.3 us)
Async XLA Ops:
  6.5 88.5 %copy-start = (bf16[2,256,256]{2,1,0:T(8,128)(2,1)S(1)}, bf16[2,256,256]{2,1,0:T(8,128)(2,1)}, u32[]{:S(2)}) copy-start(bf16[2,256,256]{2,1,0:T(8,128)(2,1)} %param.17) | copy-start | bytes 786436
  6.5 6.1 %copy-start.9 = (bf16[4,512]{1,0:T(4,128)(2,1)S(1)}, bf16[4,512]{1,0:T(4,128)(2,1)}, u32[]{:S(2)}) copy-start(bf16[4,512]{1,0:T(4,128)(2,1)} %param.16) | copy-start | bytes 12292
  6.5 29.5 %all-gather.7.cloned.1.call-start = ((), (), s32[]{:S(2)}) async-start(), calls=%async_computation.1 | async-start | bytes 2621440 | tf_op jit(solution)/shard_map/all_gather | solution.py:61
  10.6 76.7 %all-gather.9.cloned.1.call-start = ((), (), s32[]{:S(2)}) async-start(), calls=%async_computation.2 | async-start | bytes 2359296 | tf_op jit(solution)/shard_map/all_gather | solution.py:57
  11.3 233.0 %all-gather.11.cloned.1.call-start = ((), (), s32[]{:S(2)}) async-start(), calls=%async_computation.3 | async-start | bytes 2359296 | tf_op jit(solution)/shard_map/all_gather | solution.py:58
  12.1 232.3 %all-gather.13.cloned.1.call-start = ((), (), s32[]{:S(2)}) async-start(), calls=%async_computation.4 | async-start | bytes 2359296 | tf_op jit(solution)/shard_map/all_gather | solution.py:103
  12.6 268.2 %reduce-scatter.2.cloned.1.call-start = ((), (), s32[]{:S(2)}) async-start(), calls=%async_computation.5 | async-start | bytes 2621440 | tf_op jit(solution)/shard_map/reduce_scatter | solution.py:104
  12.7 80.5 %copy-start.10 = (f32[512]{0:T(512)S(1)}, f32[512]{0:T(512)}, u32[]{:S(2)}) copy-start(f32[512]{0:T(512)} %param.19) | copy-start | bytes 6148
  12.7 82.3 %copy-start.12 = (f32[2,512]{1,0:T(2,128)S(1)}, f32[2,512]{1,0:T(2,128)}, u32[]{:S(2)}) copy-start(f32[2,512]{1,0:T(2,128)} %param.20) | copy-start | bytes 12292
  90.7 3.8 %collective-permute-start = (bf16[3,512]{1,0:T(4,128)(2,1)S(1)}, bf16[3,512]{1,0:T(4,128)(2,1)S(1)}, u32[]{:S(2)}, u32[]{:S(2)}) collective-permute-start(bf16[3,512]{1,0:T(4,128)(2,1)S(1)} %slice.388), channel_id=1, source_target_pairs={{0,4},{4,8},{8,12},{12,16},{16,20},{20,24},{24,28},{1,5},{5,9},{9,... | collective-permute-start | bytes 9224 | tf_op jit(solution)/shard_map/ppermute | solution.py:13
  95.0 0.8 copy-start.2
  95.1 1.1 copy-start.11
  100.9 26.1 %copy-start.1 = (f32[512,512]{1,0:T(8,128)}, f32[512,512]{1,0:T(8,128)S(1)}, u32[]{:S(2)}) copy-start(f32[512,512]{1,0:T(8,128)S(1)} %convert_multiply_fusion.5) | copy-start | bytes 3145732
  165.9 1.3 copy-start.3
  165.9 1.4 copy-start.4
  175.5 1.1 copy-start.5
  175.5 1.2 copy-start.6
  177.8 2.9 %slice-start = ((f32[512,512]{1,0:T(8,128)}), f32[1,512]{1,0:T(1,128)S(1)}, s32[]{:S(2)}) async-start(f32[512,512]{1,0:T(8,128)} %copy-done.1), calls=%async_computation.6 | async-start | bytes 4096 | tf_op jit(solution)/shard_map/slice | solution.py:97
  177.8 2.9 %copy-start.7 = (f32[255,512]{1,0:T(8,128)S(1)}, f32[255,512]{1,0:T(8,128)}, u32[]{:S(2)}) copy-start(f32[255,512]{1,0:T(8,128)} %get-tuple-element.130) | copy-start | bytes 1566724
  180.8 36.3 %copy-start.8 = (f32[512,512]{1,0:T(8,128)S(1)}, f32[512,512]{1,0:T(8,128)}, u32[]{:S(2)}) copy-start(f32[512,512]{1,0:T(8,128)} %pad.144) | copy-start | bytes 3145732
Sparse Core Ops, SparseCore 0:
  10.7 25.2 all-gather.6
  38.1 49.0 all-gather.8
  89.4 47.6 all-gather.10
  139.0 48.8 all-gather.12
  252.4 28.3 reduce-scatter.1
where the time goes:
time: 288 us; the launch traced here: 287 us
  waiting for transfers between devices  106 us (37%)
  local copies, waits for them, and re-layouts  85.9 us (30%)
  blocking collectives  53.4 us (19%)
  between operations  14.1 us (5%)
  matrix products  13.9 us (5%)
  other arithmetic  10.9 us (4%)
    slice x61, local copies, waits for them, and re-layouts, on_device(): lax.associative_scan(combine_pair, (decay, drive), axis=0)  68.6 us
    all_gather x2, blocking collectives, carried_in(): everything = jax.tree.map(lambda part: lax.all_gather(part, axis), array)  53.4 us
    all_gather x1, waiting for transfers between devices, on_device(): lax.all_gather(proj_x, 'sp', axis=0, tiled=True)  51.2 us
    reduce_scatter x1, waiting for transfers between devices, on_device(): lax.psum_scatter(jnp.dot(mixed, out_cols, preferred_element_type=jnp.floa...  28.5 us
    all_gather x1, waiting for transfers between devices, on_device(): piece = lax.all_gather(normed, 'tp', axis=0, tiled=True)  23.3 us
    pad x32, local copies, waits for them, and re-layouts, on_device(): lax.associative_scan(combine_pair, (decay, drive), axis=0)  11.7 us
    dot_general x1, matrix products, on_device(): jnp.dot(mixed, out_cols, preferred_element_type=jnp.float32)  7.88 us
  transfers between devices with their start and end apart: 6, of which 4 were waited for; matrix products, arithmetic and copies ran while one was open for 34% of the time, Pallas kernels for 0%

commit v1 on v0

--- a/solution.py
+++ b/solution.py
@@ -1,6 +1,10 @@
+import functools
+
 import jax
 import jax.numpy as jnp
 from jax import lax
+from jax.experimental import pallas as pl
+from jax.experimental.pallas import tpu as pltpu
 from jax.sharding import PartitionSpec as P
 
 HEAD = 256
@@ -109,7 +113,397 @@
     )
 
 
+MESH = pl.DeviceIdType.MESH
+
+
+def fused(
+    nz, tok, gain, wx, wg, taps, gr, gi, dp, ds, wo, out,
+    xb, wxb, wgb, wob, bf, hs, cum, shc, dsb, mx, cs, cr, carry, psend, keep, precv, sb, acc, rb,
+    w_send, w_recv, y_send, t_send, t_recv, m_send, m_recv, c_send, c_recv, p_send, p_recv, r_send, r_recv,
+):
+    sp, tp = lax.axis_index("sp"), lax.axis_index("tp")
+    z, y = sp // 2, sp % 2
+    x, c = tp // 2, tp % 2
+    rows, width = tok.shape
+    krows, half = wx.shape[0], wx.shape[1] // 2
+    ocols = wo.shape[1]
+    f32, bf16 = jnp.float32, jnp.bfloat16
+    y2, x2, c2 = 1 - y, 1 - x, 1 - c
+    dev_c, dev_x = (sp, 2 * x + c2), (sp, 2 * x2 + c)
+    dev_y, dev_xy = (2 * z + y2, tp), (2 * z + y2, 2 * x2 + c)
+
+    def line(zz):
+        return (2 * zz + y, tp)
+
+    def remote(src, dst, ssem, rsem, device):
+        return pltpu.make_async_remote_copy(
+            src_ref=src, dst_ref=dst, send_sem=ssem, recv_sem=rsem, device_id=device, device_id_type=MESH
+        )
+
+    barrier = pltpu.get_barrier_semaphore()
+    for device in (dev_c, dev_x, dev_y, dev_xy):
+        pl.semaphore_signal(barrier, inc=1, device_id=device, device_id_type=MESH)
+    for k in range(1, nz):
+        pl.semaphore_signal(barrier, inc=1, device_id=line((z + k) % nz), device_id_type=MESH)
+
+    slot0 = y * 4 + tp
+    for part in range(4):
+        step = rows // 4
+        rs = pl.ds(part * step, step)
+        v = tok[rs, :].astype(f32)
+        v = v * lax.rsqrt(jnp.mean(v * v, axis=-1, keepdims=True) + 1e-06)
+        xb[slot0, rs, :] = (v * gain[...].astype(f32)).astype(bf16)
+
+    bufs = (wxb, wgb, wob)
+
+    def piece(w, zz, yy):
+        return bufs[w].at[pl.ds(pl.multiple_of((2 * zz + yy) * half, half), half), :]
+
+    def source(w, yy):
+        if w == 2:
+            return wo.at[pl.ds(pl.multiple_of(yy * half, half), half), :]
+        return (wx, wg)[w].at[:, pl.ds(pl.multiple_of(yy * half, half), half)]
+
+    def to_y(w):
+        return remote(source(w, y2), piece(w, z, y), y_send.at[w], w_recv.at[w, z, y], dev_y)
+
+    def from_y(w):
+        return remote(source(w, y2), piece(w, z, y2), y_send.at[w], w_recv.at[w, z, y2], dev_y)
+
+    def along(w, zz, yy, direction, src=None):
+        device = line(z + 1) if direction == 0 else line(z - 1)
+        return remote(
+            piece(w, zz, yy) if src is None else src, piece(w, zz, yy),
+            w_send.at[w, zz, yy, direction], w_recv.at[w, zz, yy], device,
+        )
+
+    def send_both(w, yy, src=None):
+        @pl.when(z + 1 < nz)
+        def _():
+            along(w, z, yy, 0, src).start()
+
+        @pl.when(z > 0)
+        def _():
+            along(w, z, yy, 1, src).start()
+
+    def own(w):
+        send_both(w, y, source(w, y))
+        piece(w, z, y)[...] = source(w, y)[...]
+        from_y(w).wait_recv()
+        send_both(w, y2)
+
+    near = jnp.minimum(z, nz - 1 - z)
+
+    def origin(u):
+        side = (z - (u + 1) // 2) if u % 2 else (z + u // 2)
+        outer = jnp.where(2 * z < nz, u, nz - 1 - u)
+        return jnp.where(u <= 2 * near, side, outer)
+
+    def arrive(w, u):
+        zz = origin(u)
+        for yy in (y, y2):
+            along(w, zz, yy, 0).wait_recv()
+
+            @pl.when(jnp.logical_and(zz < z, z + 1 < nz))
+            def _():
+                along(w, zz, yy, 0).start()
+
+            @pl.when(jnp.logical_and(zz > z, z > 0))
+            def _():
+                along(w, zz, yy, 1).start()
+
+    def slot(yy, xx, cc):
+        return yy * 4 + xx * 2 + cc
+
+    cut = rows * 3 // 4
+    top, low = pl.ds(0, cut), pl.ds(cut, rows - cut)
+
+    def token(src, dst, s, r, device):
+        return remote(src, dst, t_send.at[s], t_recv.at[r], device)
+
+    def block(yy, xx, cc):
+        return xb.at[slot(yy, xx, cc)]
+
+    def same(ref, s, r, device):
+        return token(ref, ref, s, r, device)
+
+    pl.semaphore_wait(barrier, 4 + nz - 1)
+    to_y(0).start()
+    same(block(y, x, c), 1, 0, dev_x).start()
+    same(block(y, x, c), 2, 1, dev_y).start()
+    same(block(y, x, c), 0, 4, dev_c).start()
+    shift_copy = remote(ds, dsb, m_send.at[1], m_recv.at[1], dev_y)
+    shift_copy.start()
+    to_y(1).start()
+    own(0)
+
+    shift_copy.wait_recv()
+    mine = jnp.where(y == 0, ds[0:1, :], ds[1:2, :])
+    theirs = jnp.where(y == 0, dsb[0:1, :], dsb[1:2, :])
+    first = jnp.where(y == 0, mine, theirs)
+    second = jnp.where(y == 0, theirs, mine)
+    for b in range(8):
+        row = (first, second)[b // 4][:, (b % 4) * rows : (b % 4 + 1) * rows]
+        shc[b] = jnp.broadcast_to(row, (rows, rows)).T
+
+    arrive(0, 1)
+    for u in range(2, nz - 1):
+        arrive(0, u)
+
+    @pl.when(near > 0)
+    def _():
+        arrive(0, nz - 1)
+
+    same(block(y, x2, c), 1, 0, dev_x).wait_recv()
+    same(block(y, x2, c).at[low], 3, 3, dev_y).start()
+    same(block(y, x2, c), 4, 5, dev_c).start()
+    same(block(y2, x, c), 2, 1, dev_y).wait_recv()
+    same(block(y2, x, c).at[top], 5, 2, dev_x).start()
+    same(block(y2, x, c), 6, 6, dev_c).start()
+    to_y(2).start()
+
+    @pl.when(near == 0)
+    def _():
+        arrive(0, nz - 1)
+
+    own(1)
+    same(block(y2, x2, c).at[top], 5, 2, dev_x).wait_recv()
+    same(block(y2, x2, c).at[low], 3, 3, dev_y).wait_recv()
+    same(block(y2, x2, c), 7, 7, dev_c).start()
+    same(block(y, x, c2), 0, 4, dev_c).wait_recv()
+    same(block(y, x2, c2), 4, 5, dev_c).wait_recv()
+    same(block(y2, x, c2), 6, 6, dev_c).wait_recv()
+    same(block(y2, x2, c2), 7, 7, dev_c).wait_recv()
+
+    @pl.when(z == 0)
+    def _():
+        bf[0:8, :] = jnp.zeros((8, half), f32)
+
+    @pl.loop(0, 8)
+    def _(b):
+        v = jnp.dot(xb[b], wxb[...], preferred_element_type=f32)
+        bf[pl.ds(pl.multiple_of(8 + b * rows, 8), rows), :] = v.astype(bf16).astype(f32)
+
+    def tail(device):
+        return remote(bf.at[pl.ds(8 * rows, 8), :], bf.at[pl.ds(0, 8), :], m_send.at[0], m_recv.at[0], device)
+
+    @pl.when(z + 1 < nz)
+    def _():
+        tail(line(z + 1)).start()
+
+    arrive(1, 1)
+
+    @pl.when(z > 0)
+    def _():
+        tail(line(z - 1)).wait_recv()
+
+    lanes = pl.ds(pl.multiple_of(y * half, half), half)
+    tap = taps[:, lanes].astype(f32)
+    minus = -dp[:, lanes]
+    rate = jnp.maximum(minus, 0.0) + jnp.log1p(jnp.exp(-jnp.abs(minus)))
+    index = lax.broadcasted_iota(jnp.int32, (rows, half), 0)
+
+    def shift_rows(v, s, fill):
+        if s < 8:
+            return jnp.where(index >= s, pltpu.roll(v, s, 0), fill)
+        return jnp.concatenate([jnp.full((s, half), fill, f32), v[: rows - s]], axis=0)
+
+    def recurrence(b, before):
+        window = bf[pl.ds(pl.multiple_of(b * rows, 8), rows + 8), :]
+        total = jnp.zeros((rows, half), f32)
+        for k in range(CONV):
+            lo = 8 - CONV + 1 + k
+            total = total + window[lo : lo + rows] * tap[k : k + 1]
+        conved = total.astype(bf16)
+        recur = jax.nn.sigmoid(jnp.dot(conved, gr[y], preferred_element_type=f32))
+        inlet = jax.nn.sigmoid(jnp.dot(conved, gi[y], preferred_element_type=f32))
+        shift = shc[b]
+        shift = jnp.concatenate([shift] * (half // rows), axis=1)
+        log_decay = -8.0 * recur * rate + shift
+        a = jnp.exp(log_decay)
+        t = 2.0 * log_decay
+        series = 1.0 + t * (1.0 / 9.0)
+        for k in range(8, 1, -1):
+            series = 1.0 + t * (1.0 / k) * series
+        lost = jnp.where(t > -0.5, -t * series, 1.0 - a * a)
+        h = jnp.sqrt(lost) * inlet * conved.astype(f32)
+        s = 1
+        while s < rows:
+            h = a * shift_rows(h, s, 0.0) + h
+            a = a * shift_rows(a, s, 1.0)
+            s *= 2
+        h = h + a * before[1]
+        a = a * before[0]
+        hs[b] = h
+        cum[b] = a
+        return (a[rows - 1 :], h[rows - 1 :])
+
+    state = (jnp.ones((1, half), f32), jnp.zeros((1, half), f32))
+    state = lax.fori_loop(0, 4, recurrence, state)
+    for u in range(2, nz - 1):
+        arrive(1, u)
+    state = lax.fori_loop(4, 8, recurrence, state)
+    cs[0:8, :] = jnp.broadcast_to(state[0], (8, half))
+    cs[8:16, :] = jnp.broadcast_to(state[1], (8, half))
+
+    def carries(k, zz, device):
+        return remote(cs, cr.at[zz], c_send.at[k], c_recv.at[zz], device)
+
+    for k in range(1, nz):
+        @pl.when(z + k < nz)
+        def _():
+            carries(k, z, line(z + k)).start()
+
+    arrive(1, nz - 1)
+    own(2)
+
+    @pl.when(z + 1 < nz)
+    def _():
+        tail(line(z + 1)).wait_send()
+
+    @pl.loop(0, 8)
+    def _(b):
+        v = jnp.dot(xb[b], wgb[...], preferred_element_type=f32).astype(bf16).astype(f32)
+        inner = 0.7978845608028654 * (v + 0.044715 * (v * v * v))
+        bf[pl.ds(pl.multiple_of(8 + b * rows, 8), rows), :] = 0.5 * v * (1.0 + jnp.tanh(inner))
+
+    carry[...] = jnp.zeros((8, half), f32)
+    for k in range(nz - 1):
+        @pl.when(k < z)
+        def _():
+            carries(0, k, dev_y).wait_recv()
+            carry[...] = cr[k, 0:8, :] * carry[...] + cr[k, 8:16, :]
+
+    @pl.loop(0, 8)
+    def _(b):
+        gate = bf[pl.ds(pl.multiple_of(8 + b * rows, 8), rows), :]
+        mx[b] = ((hs[b] + cum[b] * carry[0:1, :]) * gate).astype(bf16)
+
+    def partial(u):
+        zz = origin(u)
+
+        @pl.loop(0, 4)
+        def _(q):
+            for yy in range(2):
+                cols = pl.ds(yy * ocols, ocols)
+                weights = piece(2, zz, yy)[...]
+                psend[u, q, :, cols] = jnp.dot(mx[2 * q + c2], weights, preferred_element_type=f32).astype(bf16)
+
+        exchange(u).start()
+
+        @pl.loop(0, 4)
+        def _(q):
+            for yy in range(2):
+                cols = pl.ds(yy * ocols, ocols)
+                weights = piece(2, zz, yy)[...]
+                keep[u, q, :, cols] = jnp.dot(mx[2 * q + c], weights, preferred_element_type=f32)
+
+    def exchange(u):
+        return remote(psend.at[u], precv.at[u], p_send.at[u], p_recv.at[u], dev_c)
+
+    def spread(u, r):
+        return remote(sb.at[u, r], rb.at[u, r], r_send.at[u, r], r_recv.at[u, r], (dev_x, dev_y, dev_xy)[r])
+
+    def pair_sum(u):
+        exchange(u).wait_recv()
+        for r, q in enumerate((2 * y + x2, 2 * y2 + x, 2 * y2 + x2)):
+            sb[u, r] = (keep[u, q] + precv[u, q].astype(f32)).astype(bf16)
+            spread(u, r).start()
+        q = 2 * y + x
+        acc[u] = keep[u, q] + precv[u, q].astype(f32)
+
+    def finish(u):
+        total = acc[u]
+        for r in range(3):
+            spread(u, r).wait_recv()
+            total = total + rb[u, r].astype(f32)
+        out[:, pl.ds(pl.multiple_of(origin(u) * 2 * ocols, ocols), 2 * ocols)] = total.astype(bf16)
+
+    for u in range(nz):
+        if u:
+            arrive(2, u)
+        partial(u)
+        if u:
+            pair_sum(u - 1)
+    for u in range(nz - 2):
+        finish(u)
+    pair_sum(nz - 1)
+    for u in range(max(nz - 2, 0), nz):
+        finish(u)
+
+    for w in range(3):
+        to_y(w).wait_send()
+        for zz in range(nz):
+            for yy in range(2):
+                @pl.when(jnp.logical_and(zz <= z, z + 1 < nz))
+                def _():
+                    along(w, zz, yy, 0).wait_send()
+
+                @pl.when(jnp.logical_and(zz >= z, z > 0))
+                def _():
+                    along(w, zz, yy, 1).wait_send()
+    full = block(y, x, c)
+    for s, ref in enumerate((full, full, full, full.at[low], full, full.at[top], full, full)):
+        same(ref, s, 0, dev_c).wait_send()
+    shift_copy.wait_send()
+
+    for k in range(1, nz):
+        @pl.when(z + k < nz)
+        def _():
+            carries(k, z, line(z + k)).wait_send()
+    for u in range(nz):
+        exchange(u).wait_send()
+        for r in range(3):
+            spread(u, r).wait_send()
+
+
+def fused_on_device(
+    nz, tokens, norm_gain, proj_x, gate_projection, conv_taps, gate_recur, gate_input, decay_param, decay_shift, proj_out
+):
+    rows, width = tokens.shape
+    half = proj_x.shape[1] // 2
+    ocols = proj_out.shape[1]
+    bf16, f32 = jnp.bfloat16, jnp.float32
+    dma = pltpu.SemaphoreType.DMA
+    return pl.pallas_call(
+        functools.partial(fused, nz),
+        out_shape=jax.ShapeDtypeStruct((rows, width), bf16),
+        in_specs=[pl.BlockSpec(memory_space=pltpu.VMEM)] * 10,
+        out_specs=pl.BlockSpec(memory_space=pltpu.VMEM),
+        scratch_shapes=[
+            pltpu.VMEM((8, rows, width), bf16),
+            pltpu.VMEM((2 * nz * half, half), bf16),
+            pltpu.VMEM((2 * nz * half, half), bf16),
+            pltpu.VMEM((2 * nz * half, ocols), bf16),
+            pltpu.VMEM((8 * rows + 8, half), f32),
+            pltpu.VMEM((8, rows, half), f32),
+            pltpu.VMEM((8, rows, half), f32),
+            pltpu.VMEM((8, rows, rows), f32),
+            pltpu.VMEM(decay_shift.shape, f32),
+            pltpu.VMEM((8, rows, half), bf16),
+            pltpu.VMEM((16, half), f32),
+            pltpu.VMEM((nz, 16, half), f32),
+            pltpu.VMEM((8, half), f32),
+            pltpu.VMEM((nz, 4, rows, 2 * ocols), bf16),
+            pltpu.VMEM((nz, 4, rows, 2 * ocols), f32),
+            pltpu.VMEM((nz, 4, rows, 2 * ocols), bf16),
+            pltpu.VMEM((nz, 3, rows, 2 * ocols), bf16),
+            pltpu.VMEM((nz, rows, 2 * ocols), f32),
+            pltpu.VMEM((nz, 3, rows, 2 * ocols), bf16),
+            dma((3, nz, 2, 2)), dma((3, nz, 2)), dma((3,)), dma((8,)), dma((8,)), dma((2,)), dma((2,)),
+            dma((nz,)), dma((nz,)), dma((nz,)), dma((nz,)), dma((nz, 3)), dma((nz, 3)),
+        ],
+        compiler_params=pltpu.CompilerParams(
+            collective_id=0, has_side_effects=True, vmem_limit_bytes=56 * 1024 * 1024
+        ),
+    )(
+        tokens, norm_gain.reshape(1, width), proj_x, gate_projection, conv_taps, gate_recur, gate_input,
+        decay_param.reshape(1, -1), decay_shift, proj_out,
+    )
+
+
 def solution(mesh):
+    n_sp, n_tp = mesh.shape["sp"], mesh.shape["tp"]
     in_specs = (
         P(("sp", "tp"), None),
         P(),
@@ -123,6 +517,13 @@
         P("tp", "sp"),
     )
     out_specs = P(("sp", "tp"), None)
+    small = n_tp == 4 and n_sp % 2 == 0 and 4 <= n_sp <= 8
+
+    def body(*args):
+        rows, heads, krows, ocols = args[0].shape[0], args[5].shape[0], args[2].shape[0], args[9].shape[1]
+        fits = heads == 2 and krows == HEAD and ocols == HEAD and args[8].shape[1] == 4 * rows and rows == HEAD // 2
+        return fused_on_device(n_sp // 2, *args) if small and fits else on_device(*args)
+
     return jax.shard_map(
-        on_device, mesh=mesh, in_specs=in_specs, out_specs=out_specs, check_vma=False
-    )
+        body, mesh=mesh, in_specs=in_specs, out_specs=out_specs, check_vma=False
+    )

time: 288 us -> 102 us (0.35)
  waiting for transfers between devices: 106 us -> 0 us
  Pallas kernels: 0 us -> 98.7 us
  local copies, waits for them, and re-layouts: 85.9 us -> 3.17 us
  blocking collectives: 53.4 us -> 0 us
  between operations: 14.1 us -> 0.01 us
  matrix products: 13.9 us -> 0 us
  other arithmetic: 10.9 us -> 0 us
    pallas_call x0 -> x1, Pallas kernels: none -> 98.7 us  [fused_on_device(): pl.pallas_call(functools.partial(fused, nz), out_shape=jax.ShapeDtypeStru...]
    all_gather x4 -> x0, waiting for transfers between devices: 74.6 us -> none  [the longest x1 51.2 us: on_device(): lax.all_gather(proj_x, 'sp', axis=0, tiled=True)]
    slice x62 -> x0, local copies, waits for them, and re-layouts: 68.6 us -> none  [the longest x61 68.6 us: on_device(): lax.associative_scan(combine_pair, (decay, drive), axis=0)]
    all_gather x2 -> x0, blocking collectives: 53.4 us -> none  [carried_in(): everything = jax.tree.map(lambda part: lax.all_gather(part, axis), array)]
    reduce_scatter x1 -> x0, waiting for transfers between devices: 28.5 us -> none  [on_device(): lax.psum_scatter(jnp.dot(mixed, out_cols, preferred_element_type=jnp.floa...]
    dot_general x4 -> x0, matrix products: 13.9 us -> none  [the longest x1 7.88 us: on_device(): jnp.dot(mixed, out_cols, preferred_element_type=jnp.float32)]
    pad x32 -> x0, local copies, waits for them, and re-layouts: 11.7 us -> none  [on_device(): lax.associative_scan(combine_pair, (decay, drive), axis=0)]
    add x31 -> x0, other arithmetic: 3.25 us -> none  [the longest x16 2.9 us: combine_pair(): return (earlier[0] * later[0], later[0] * earlier[1] + later[1])]
  transfers between devices with their start and end apart: 6 -> 0, of which waited for: 4 -> 0; matrix products, arithmetic and copies ran while one was open for 34% -> 0% of each run, Pallas kernels for 0% -> 0%
where the time goes in v1:
time: 102 us
  Pallas kernels  98.7 us (97%)
  local copies, waits for them, and re-layouts  3.17 us (3%)
    pallas_call x1, Pallas kernels, fused_on_device(): pl.pallas_call(functools.partial(fused, nz), out_shape=jax.ShapeDtypeStru...  98.7 us

profile of v1, /device:TPU:0, one launch (start us, length us, event | category | flops | bytes accessed | tf_op | source)
XLA Modules:
  0.0 101.9 jit_solution(2468407185365018282)
XLA Ops:
  0.0 1.3 %reshape.6.gain = bf16[1,2048]{1,0:T(2,128)(2,1)} reshape(bf16[2048]{0:T(1024)(128)(2,1)} %param.11) | data formatting | bytes 8192 | tf_op jit(solution)/shard_map/reshape | solution.py:500
  1.3 98.7 %shard_map.100 = bf16[128,2048]{1,0:T(8,128)(2,1)} custom-call(bf16[128,2048]{1,0:T(8,128)(2,1)} %tok.1, bf16[1,2048]{1,0:T(2,128)(2,1)} %reshape.6.gain, bf16[256,512]{1,0:T(8,128)(2,1)} %wx.1, bf16[256,512]{1,0:T(8,128)(2,1)} %wg.1, bf16[4,512]{1,0:T(4,128)(2,1)} %taps.1, bf16[2,256,256]{2,1,0:T(8,128)(2,1)} %gr.1, bf16[2,256,256]{2,1,0:T(8,128)(2,1)} %gi.1, ...), custom_call_target="tpu_custom_call" | custom-call | tf_op jit(solution)/shard_map/pallas_call | solution.py:468
  100.0 1.9 %copy.12 = bf16[128,2048]{1,0:T(8,128)(2,1)} copy(bf16[128,2048]{1,0:T(8,128)(2,1)} %shard_map.100) | data formatting | bytes 1048576

commit v2 on v1

--- a/solution.py
+++ b/solution.py
@@ -267,11 +267,17 @@
         arrive(0, nz - 1)
 
     own(1)
+    same(block(y, x, c2), 0, 4, dev_c).wait_recv()
+    same(block(y, x2, c2), 4, 5, dev_c).wait_recv()
+
+    def project(part):
+        v = jnp.dot(xb[pl.ds(4 * part, 4)].reshape(4 * rows, width), wxb[...], preferred_element_type=f32)
+        bf[pl.ds(pl.multiple_of(8 + part * 4 * rows, 8), 4 * rows), :] = v.astype(bf16).astype(f32)
+
+    project(y)
     same(block(y2, x2, c).at[top], 5, 2, dev_x).wait_recv()
     same(block(y2, x2, c).at[low], 3, 3, dev_y).wait_recv()
     same(block(y2, x2, c), 7, 7, dev_c).start()
-    same(block(y, x, c2), 0, 4, dev_c).wait_recv()
-    same(block(y, x2, c2), 4, 5, dev_c).wait_recv()
     same(block(y2, x, c2), 6, 6, dev_c).wait_recv()
     same(block(y2, x2, c2), 7, 7, dev_c).wait_recv()
 
@@ -279,10 +285,7 @@
     def _():
         bf[0:8, :] = jnp.zeros((8, half), f32)
 
-    @pl.loop(0, 8)
-    def _(b):
-        v = jnp.dot(xb[b], wxb[...], preferred_element_type=f32)
-        bf[pl.ds(pl.multiple_of(8 + b * rows, 8), rows), :] = v.astype(bf16).astype(f32)
+    project(y2)
 
     def tail(device):
         return remote(bf.at[pl.ds(8 * rows, 8), :], bf.at[pl.ds(0, 8), :], m_send.at[0], m_recv.at[0], device)
@@ -361,9 +364,14 @@
     def _():
         tail(line(z + 1)).wait_send()
 
+    @pl.loop(0, 2)
+    def _(part):
+        v = jnp.dot(xb[pl.ds(4 * part, 4)].reshape(4 * rows, width), wgb[...], preferred_element_type=f32)
+        bf[pl.ds(pl.multiple_of(8 + part * 4 * rows, 8), 4 * rows), :] = v.astype(bf16).astype(f32)
+
     @pl.loop(0, 8)
     def _(b):
-        v = jnp.dot(xb[b], wgb[...], preferred_element_type=f32).astype(bf16).astype(f32)
+        v = bf[pl.ds(pl.multiple_of(8 + b * rows, 8), rows), :]
         inner = 0.7978845608028654 * (v + 0.044715 * (v * v * v))
         bf[pl.ds(pl.multiple_of(8 + b * rows, 8), rows), :] = 0.5 * v * (1.0 + jnp.tanh(inner))
 
@@ -377,26 +385,20 @@
     @pl.loop(0, 8)
     def _(b):
         gate = bf[pl.ds(pl.multiple_of(8 + b * rows, 8), rows), :]
-        mx[b] = ((hs[b] + cum[b] * carry[0:1, :]) * gate).astype(bf16)
+        mx[b % 2, b // 2] = ((hs[b] + cum[b] * carry[0:1, :]) * gate).astype(bf16)
 
     def partial(u):
         zz = origin(u)
 
-        @pl.loop(0, 4)
-        def _(q):
-            for yy in range(2):
-                cols = pl.ds(yy * ocols, ocols)
-                weights = piece(2, zz, yy)[...]
-                psend[u, q, :, cols] = jnp.dot(mx[2 * q + c2], weights, preferred_element_type=f32).astype(bf16)
-
+        def product(core, yy):
+            values = mx[core].reshape(4 * rows, half)
+            return jnp.dot(values, piece(2, zz, yy)[...], preferred_element_type=f32).reshape(4, rows, ocols)
+
+        for yy in range(2):
+            psend[u, :, :, yy * ocols : (yy + 1) * ocols] = product(c2, yy).astype(bf16)
         exchange(u).start()
-
-        @pl.loop(0, 4)
-        def _(q):
-            for yy in range(2):
-                cols = pl.ds(yy * ocols, ocols)
-                weights = piece(2, zz, yy)[...]
-                keep[u, q, :, cols] = jnp.dot(mx[2 * q + c], weights, preferred_element_type=f32)
+        for yy in range(2):
+            keep[u, :, :, yy * ocols : (yy + 1) * ocols] = product(c, yy)
 
     def exchange(u):
         return remote(psend.at[u], precv.at[u], p_send.at[u], p_recv.at[u], dev_c)
@@ -480,7 +482,7 @@
             pltpu.VMEM((8, rows, half), f32),
             pltpu.VMEM((8, rows, rows), f32),
             pltpu.VMEM(decay_shift.shape, f32),
-            pltpu.VMEM((8, rows, half), bf16),
+            pltpu.VMEM((2, 4, rows, half), bf16),
             pltpu.VMEM((16, half), f32),
             pltpu.VMEM((nz, 16, half), f32),
             pltpu.VMEM((8, half), f32),

time: 102 us -> 99.1 us (0.972)
  Pallas kernels: 98.7 us -> 95.7 us
    pallas_call x1, Pallas kernels: 98.7 us -> 95.7 us  [fused_on_device(): pl.pallas_call(functools.partial(fused, nz), out_shape=jax.ShapeDtypeStru...]
where the time goes in v2:
time: 99.1 us; the launch traced here: 98.9 us
  Pallas kernels  95.7 us (97%)
  local copies, waits for them, and re-layouts  3.17 us (3%)
    pallas_call x1, Pallas kernels, fused_on_device(): pl.pallas_call(functools.partial(fused, nz), out_shape=jax.ShapeDtypeStru...  95.7 us

profile of v2, /device:TPU:0, one launch (start us, length us, event | category | flops | bytes accessed | tf_op | source)
XLA Modules:
  0.0 98.9 jit_solution(7710485897803931149)
XLA Ops:
  0.0 1.3 %reshape.6.gain = bf16[1,2048]{1,0:T(2,128)(2,1)} reshape(bf16[2048]{0:T(1024)(128)(2,1)} %param.11) | data formatting | bytes 8192 | tf_op jit(solution)/shard_map/reshape | solution.py:502
  1.3 95.7 %shard_map.100 = bf16[128,2048]{1,0:T(8,128)(2,1)} custom-call(bf16[128,2048]{1,0:T(8,128)(2,1)} %tok.1, bf16[1,2048]{1,0:T(2,128)(2,1)} %reshape.6.gain, bf16[256,512]{1,0:T(8,128)(2,1)} %wx.1, bf16[256,512]{1,0:T(8,128)(2,1)} %wg.1, bf16[4,512]{1,0:T(4,128)(2,1)} %taps.1, bf16[2,256,256]{2,1,0:T(8,128)(2,1)} %gr.1, bf16[2,256,256]{2,1,0:T(8,128)(2,1)} %gi.1, ...), custom_call_target="tpu_custom_call" | custom-call | tf_op jit(solution)/shard_map/pallas_call | solution.py:470
  97.0 1.9 %copy.12 = bf16[128,2048]{1,0:T(8,128)(2,1)} copy(bf16[128,2048]{1,0:T(8,128)(2,1)} %shard_map.100) | data formatting | bytes 1048576
